TPU v7x, 32 devices: a whole 2x2x4 slice. The times are simulated.
32 devices in a mesh: sp: 4 (over y, x), dp: 8 (over z, core).
Axes of the slice: x: 2, y: 2, z: 4, core: 2. Of those that a mesh axis runs over, the one named last changes fastest.
Arguments:
- value_half: bfloat16 [8, 1024, 2048], P('dp', 'sp'), may hold values from -6 to 6
- gate_half: bfloat16 [8, 1024, 2048], P('dp', 'sp'), may hold values from -6 to 6
- upstream: bfloat16 [8, 1024, 2048], P('dp', 'sp'), may hold values from -6 to 6
- conv_taps: float32 [31, 2048], P(None, 'sp'), may hold values from -1 to 1
- norm_gain: float32 [2048], replicated, may hold values from 0.1 to 1.9
- out_weight: bfloat16 [2048, 2048], P('dp'), may hold values from -0.125 to 0.125
Outputs:
- grad_value: bfloat16 [8, 1024, 2048], P('dp', 'sp')
- grad_gate: bfloat16 [8, 1024, 2048], P('dp', 'sp')
- grad_taps: float32 [31, 2048], P(None, 'sp')
- grad_gain: float32 [2048], replicated
- grad_weight: float32 [2048, 2048], P('dp')
All inputs are finite; a program needn't handle non-finite values.
Results may differ from a plain program's by a relative error of at most 0.0062.
Values may be sent and summed in bfloat16 or wider, within the bound.
A program may use at most 128 MiB of HBM per device.

v0:
```python
import jax
import jax.numpy as jnp
from jax import lax
from jax.sharding import PartitionSpec as P

NORM_EPS = 1e-05


def body(value_half, gate_half, upstream, conv_taps, norm_gain, out_weight):
    tap_count = conv_taps.shape[0]
    sig_gate = jax.nn.sigmoid(gate_half.astype(jnp.float32))
    value_wide = value_half.astype(jnp.float32)
    glu = (value_wide * sig_gate).astype(jnp.bfloat16)
    glu_heads = lax.all_to_all(glu, "sp", split_axis=2, concat_axis=1, tiled=True).astype(
        jnp.float32
    )
    length = glu_heads.shape[1]
    padded = jnp.pad(glu_heads, ((0, 0), (tap_count - 1, 0), (0, 0)))
    conv_out = jnp.zeros_like(glu_heads)
    for offset in range(tap_count):
        conv_out = conv_out + conv_taps[offset] * padded[:, offset : offset + length]
    conv_tokens = lax.all_to_all(
        conv_out.astype(jnp.bfloat16), "sp", split_axis=1, concat_axis=2, tiled=True
    ).astype(jnp.float32)
    row_mean = jnp.mean(conv_tokens, axis=-1, keepdims=True)
    centered = conv_tokens - row_mean
    inv_scale = lax.rsqrt(jnp.mean(centered * centered, axis=-1, keepdims=True) + NORM_EPS)
    normed = centered * inv_scale
    scaled = normed * norm_gain
    sig_scaled = jax.nn.sigmoid(scaled)
    activated = (scaled * sig_scaled).astype(jnp.bfloat16)[0]
    upstream_rows = upstream[0]
    columns = upstream_rows
    grad_act = jnp.dot(
        columns,
        lax.all_gather(out_weight, "dp", axis=0, tiled=True),
        preferred_element_type=jnp.float32,
    )
    grad_scaled = grad_act[None] * sig_scaled * (1.0 + scaled * (1.0 - sig_scaled))
    gain_part = jnp.sum(grad_scaled * normed, axis=(0, 1))
    grad_normed = grad_scaled * norm_gain
    grad_conv_out = inv_scale * (
        grad_normed
        - jnp.mean(grad_normed, axis=-1, keepdims=True)
        - normed * jnp.mean(grad_normed * normed, axis=-1, keepdims=True)
    )
    grad_heads = lax.all_to_all(
        grad_conv_out.astype(jnp.bfloat16), "sp", split_axis=2, concat_axis=1, tiled=True
    ).astype(jnp.float32)
    grad_padded = jnp.pad(grad_heads, ((0, 0), (0, tap_count - 1), (0, 0)))
    grad_glu = jnp.zeros_like(grad_heads)
    tap_terms = []
    for offset in range(tap_count):
        first = tap_count - 1 - offset
        grad_glu = grad_glu + conv_taps[offset] * grad_padded[:, first : first + length]
        tap_terms.append(jnp.sum(grad_heads * padded[:, offset : offset + length], axis=(0, 1)))
    grad_taps = lax.psum(jnp.stack(tap_terms), "dp")
    grad_tokens = lax.all_to_all(
        grad_glu.astype(jnp.bfloat16), "sp", split_axis=1, concat_axis=2, tiled=True
    ).astype(jnp.float32)
    grad_value = (grad_tokens * sig_gate).astype(jnp.bfloat16)
    grad_gate = (grad_tokens * value_wide * sig_gate * (1.0 - sig_gate)).astype(jnp.bfloat16)
    grad_gain = lax.psum(gain_part, ("sp", "dp"))
    columns = upstream_rows
    owned = lax.psum_scatter(
        lax.dot_general(
            columns, activated, (((0,), (0,)), ((), ())), preferred_element_type=jnp.float32
        ),
        "dp",
        scatter_dimension=0,
        tiled=True,
    )
    grad_weight = lax.psum(owned, "sp")
    return (grad_value, grad_gate, grad_taps, grad_gain, grad_weight)


def solution(mesh):
    placed = (
        P("dp", "sp", None),
        P("dp", "sp", None),
        P("dp", "sp", None),
        P(None, "sp"),
        P(),
        P("dp", None),
    )
    return jax.shard_map(
        body,
        mesh=mesh,
        in_specs=placed,
        out_specs=(P("dp", "sp", None), P("dp", "sp", None), P(None, "sp"), P(), P("dp", None)),
        check_vma=False,
    )
```

profile of v0, /device:TPU:0, one launch (start us, length us, event | category | flops | bytes accessed | tf_op | source)
XLA Modules:
  0.0 395.5 jit_solution(13518251392995277205)
XLA Ops:
  11.9 12.9 %copy.90 = bf16[1,256,2048]{1,0,2:T(2,128)(2,1)} copy(bf16[1,256,2048]{1,2,0:T(8,128)(2,1)S(1)} %fusion.1) | data formatting | bytes 2097152 | tf_op jit(solution)/shard_map/convert_element_type | solution.py:13
  25.3 11.6 %reduce.17 = bf16[2048,256]{1,0:T(8,128)(2,1)S(1)} reduce(bf16[2048,1,256]{2,1,0:T(2,128)(2,1)} %bitcast.178, bf16[]{:T(256)} %broadcast.201), dimensions={1}, to_apply=%bitcast.161.reduce_sub_computation | reduce | bytes 2097154
  38.6 5.4 %all-to-all-start = ((bf16[4,2,65536]{2,1,0:T(2,128)(2,1)}), bf16[4,2,65536]{2,1,0:T(2,128)(2,1)}, u32[]{:S(2)}, u32[]{:S(2)}) async-start(bf16[4,2,65536]{2,1,0:T(2,128)(2,1)} %reshape.389), calls=%async_computation | async-start | bytes 2097152 | tf_op jit(solution)/shard_map/all_to_all | solution.py:14
  44.1 14.2 %all-to-all-done = bf16[4,2,65536]{2,1,0:T(2,128)(2,1)} async-done(((bf16[4,2,65536]{2,1,0:T(2,128)(2,1)}), bf16[4,2,65536]{2,1,0:T(2,128)(2,1)}, u32[]{:S(2)}, u32[]{:S(2)}) %all-to-all-start) | async-done | bytes 1048608 | tf_op jit(solution)/shard_map/all_to_all | solution.py:14
  58.3 2.6 reshape.390
  64.9 8.0 %add_convert_fusion.1 = bf16[1,1024,512]{2,1,0:T(8,128)(2,1)S(1)} fusion(f32[1,1024,512]{2,1,0:T(8,128)S(1)} %bitcast.163, f32[512]{0:T(512)S(1)} %bitcast.207, f32[512]{0:T(512)S(1)} %bitcast.209, f32[512]{0:T(512)S(1)} %bitcast.213, f32[512]{0:T(512)S(1)} %bitcast.215, f32[512]{0:T(512)S(1)} %bitcast.217, f32[512]{0:T(512)S(1)} %bitcast.219, ...), kind=kLoop, calls=%fused_computation.88 | loop fusion | flops 32505856 | bytes 3209216 | tf_op jit(solution)/shard_map/convert_element_type | solution.py:23
  72.9 2.9 copy.89
  75.8 8.1 %reduce.18 = bf16[1024,512]{1,0:T(8,128)(2,1)S(1)} reduce(bf16[1024,1,512]{2,1,0:T(2,128)(2,1)} %bitcast.180, bf16[]{:T(256)} %broadcast.201), dimensions={1}, to_apply=%bitcast.160.reduce_sub_computation | reduce | bytes 2097154
  83.9 2.0 reshape.391
  85.9 4.3 %all-to-all-start.1 = ((bf16[4,2,65536]{2,1,0:T(2,128)(2,1)}), bf16[4,2,65536]{2,1,0:T(2,128)(2,1)}, u32[]{:S(2)}, u32[]{:S(2)}) async-start(bf16[4,2,65536]{2,1,0:T(2,128)(2,1)} %reshape.391), calls=%async_computation.1 | async-start | bytes 2097152 | tf_op jit(solution)/shard_map/all_to_all | solution.py:22
  90.2 13.4 %all-to-all-done.1 = bf16[4,2,65536]{2,1,0:T(2,128)(2,1)} async-done(((bf16[4,2,65536]{2,1,0:T(2,128)(2,1)}), bf16[4,2,65536]{2,1,0:T(2,128)(2,1)}, u32[]{:S(2)}, u32[]{:S(2)}) %all-to-all-start.1) | async-done | bytes 1048608 | tf_op jit(solution)/shard_map/all_to_all | solution.py:22
  103.6 3.0 reshape.392
  115.4 2.3 copy.71
  117.6 9.3 %convolution_bitcast_fusion = f32[2048,2048]{0,1:T(8,128)} fusion(bf16[256,2048]{0,1:T(8,128)(2,1)} %bitcast.186, bf16[1,256,2048]{2,1,0:T(8,128)(2,1)S(1)} %copy-done), kind=kOutput, calls=%fused_computation | convolution fusion | flops 2147483648 | bytes 18874368 | tf_op jit(solution)/shard_map/dot_general | solution.py:66
  129.2 5.7 %multiply_reduce_fusion = (f32[2048]{0:T(1024)S(1)}, f32[256]{0:T(256)S(1)}, f32[256]{0:T(256)S(1)}, f32[256,2048]{1,0:T(8,128)S(1)}) fusion(f32[256,2048]{1,0:T(8,128)S(1)} %bitcast.176, f32[256]{0:T(256)S(1)} %broadcast_multiply_fusion.2, f32[256]{0:T(256)S(1)} %add_rsqrt_fusion, f32[2048]{0:T(1024)S(1)} %copy-done.11, ...), kind=kOutput, calls=%fused_computation.20 | convolution fusion | flops 2156393984 | bytes 13651968 | tf_op jit(solution)/shard_map/dot_general | solution.py:34
  137.4 10.8 %reduce.19 = bf16[2048,256]{1,0:T(8,128)(2,1)S(1)} reduce(bf16[2048,1,256]{2,1,0:T(2,128)(2,1)S(1)} %bitcast.182, bf16[]{:T(256)} %broadcast.201), dimensions={1}, to_apply=%bitcast.148.reduce_sub_computation | reduce | bytes 2097154
  149.8 3.5 all-to-all-start.2
  153.4 48.8 %psum.22 = f32[2048]{0:T(1024)} all-reduce(f32[2048]{0:T(1024)S(1)} %get-tuple-element.35), channel_id=1, replica_groups=mesh['sp'=4,'dp'=8] {'sp','dp'}, use_global_device_ids=true, to_apply=%region_39.40 | all-reduce | flops 2048 | bytes 16384 | tf_op jit(solution)/shard_map/psum | solution.py:63
  207.1 8.0 %add_convert_fusion = bf16[1,1024,512]{2,1,0:T(8,128)(2,1)S(1)} fusion(f32[1,1024,512]{2,1,0:T(8,128)S(1)} %bitcast.162, f32[512]{0:T(512)S(1)} %bitcast.208, f32[512]{0:T(512)S(1)} %bitcast.210, f32[512]{0:T(512)S(1)} %bitcast.214, f32[512]{0:T(512)S(1)} %bitcast.216, f32[512]{0:T(512)S(1)} %bitcast.218, f32[512]{0:T(512)S(1)} %bitcast.220, ...), kind=kLoop, calls=%fused_computation.52 | loop fusion | flops 32505856 | bytes 3209216 | tf_op jit(solution)/shard_map/convert_element_type | solution.py:59
  215.0 81.4 %reduce-scatter.2.cloned.1.call-done = f32[256,2048]{0,1:T(8,128)} async-done(((f32[2048,2048]{0,1:T(8,128)}), f32[256,2048]{0,1:T(8,128)}) %reduce-scatter.2.cloned.1.call-update) | async-done | bytes 2097168 | tf_op jit(solution)/shard_map/reduce_scatter | solution.py:65
  296.5 17.9 %multiply_reduce_fusion.2 = (f32[512]{0:T(512)S(1)}, f32[512]{0:T(512)S(1)}, f32[512]{0:T(512)S(1)}, f32[512]{0:T(512)S(1)}, f32[512]{0:T(512)S(1)}, /*index=5*/...) fusion(f32[1,1024,512]{2,1,0:T(8,128)} %bitcast.164, ...), kind=kLoop, calls=%fused_computation.22 | loop fusion | flops 18865152 | bytes 4231168 | tf_op jit(solution)/shard_map/reduce_sum | solution.py:56
  314.4 2.9 copy.88
  317.4 8.0 %reduce.20 = bf16[1024,512]{1,0:T(8,128)(2,1)S(1)} reduce(bf16[1024,1,512]{2,1,0:T(2,128)(2,1)} %bitcast.179, bf16[]{:T(256)} %broadcast.201), dimensions={1}, to_apply=%bitcast.159.reduce_sub_computation | reduce | bytes 2097154
  325.4 2.0 reshape.395
  327.4 3.7 all-to-all-start.3
  331.1 2.6 multiply_reduce_fusion.1
  333.7 11.8 %multiply_reduce_fusion.3 = (f32[512]{0:T(512)S(1)}, f32[512]{0:T(512)S(1)}, f32[512]{0:T(512)S(1)}, f32[512]{0:T(512)S(1)}, f32[512]{0:T(512)S(1)}, /*index=5*/...) fusion(f32[1,1024,512]{2,1,0:T(8,128)} %bitcast.165, ...), kind=kLoop, calls=%fused_computation.23 | loop fusion | flops 12576768 | bytes 4218880 | tf_op jit(solution)/shard_map/reduce_sum | solution.py:56
  345.7 27.2 %psum.21 = f32[31,512]{1,0:T(8,128)} all-reduce(f32[31,512]{1,0:T(8,128)S(1)} %stack.127), channel_id=1, replica_groups=mesh['sp'=4,'dp'=8] {'dp'}, use_global_device_ids=true, to_apply=%region_37.38 | all-reduce | flops 15872 | bytes 126976 | tf_op jit(solution)/shard_map/psum | solution.py:57
  375.7 3.0 copy.70
  378.8 3.4 fusion.4
  382.1 2.3 copy.72
  385.8 2.9 copy.74
  (69 shorter events, 35.3 us)
Async XLA Ops:
  7.2 110.5 %copy-start = (bf16[1,256,2048]{2,1,0:T(8,128)(2,1)S(1)}, bf16[1,256,2048]{2,1,0:T(8,128)(2,1)}, u32[]{:S(2)}) copy-start(bf16[1,256,2048]{2,1,0:T(8,128)(2,1)} %param.8) | copy-start | bytes 3145732
  7.2 122.0 %all-gather.2.cloned.1.call-start = ((), (), s32[]{:S(2)}) async-start(), calls=%async_computation.5 | async-start | bytes 9437184 | tf_op jit(solution)/shard_map/all_gather | solution.py:36
  9.4 2.5 copy-start.6
  11.3 13.5 %copy-start.8 = (bf16[1,256,2048]{1,2,0:T(8,128)(2,1)}, bf16[1,256,2048]{1,2,0:T(8,128)(2,1)S(1)}, u32[]{:S(2)}) copy-start(bf16[1,256,2048]{1,2,0:T(8,128)(2,1)S(1)} %copy.57) | copy-start | bytes 3145732
  37.0 7.1 %copy-start.10 = (f32[31,512]{1,0:T(8,128)S(1)}, f32[31,512]{1,0:T(8,128)}, u32[]{:S(2)}) copy-start(f32[31,512]{1,0:T(8,128)} %param.9) | copy-start | bytes 190468
  38.6 19.7 %all-to-all-start = ((bf16[4,2,65536]{2,1,0:T(2,128)(2,1)}), bf16[4,2,65536]{2,1,0:T(2,128)(2,1)}, u32[]{:S(2)}, u32[]{:S(2)}) async-start(bf16[4,2,65536]{2,1,0:T(2,128)(2,1)} %reshape.389), calls=%async_computation | async-start | bytes 2097152 | tf_op jit(solution)/shard_map/all_to_all | solution.py:14
  60.9 2.0 copy-start.3
  64.9 10.9 %copy-start.2 = (f32[1,4,256,512]{3,2,1,0:T(8,128)}, f32[1,4,256,512]{3,2,1,0:T(8,128)S(1)}, u32[]{:S(2)}) copy-start(f32[1,4,256,512]{3,2,1,0:T(8,128)S(1)} %copy.60) | copy-start | bytes 6291460
  83.9 6.3 %copy-start.11 = (f32[2048]{0:T(1024)S(1)}, f32[2048]{0:T(1024)}, u32[]{:S(2)}) copy-start(f32[2048]{0:T(1024)} %param.10) | copy-start | bytes 24580
  85.9 17.7 %all-to-all-start.1 = ((bf16[4,2,65536]{2,1,0:T(2,128)(2,1)}), bf16[4,2,65536]{2,1,0:T(2,128)(2,1)}, u32[]{:S(2)}, u32[]{:S(2)}) async-start(bf16[4,2,65536]{2,1,0:T(2,128)(2,1)} %reshape.391), calls=%async_computation.1 | async-start | bytes 2097152 | tf_op jit(solution)/shard_map/all_to_all | solution.py:22
  90.2 206.3 %reduce-scatter.2.cloned.1.call-start = ((), (), s32[]{:S(2)}) async-start(), calls=%async_computation.6 | async-start | bytes 18874368 | tf_op jit(solution)/shard_map/reduce_scatter | solution.py:65
  106.6 1.3 copy-start.5
  149.8 52.3 %all-to-all-start.2 = ((bf16[4,2,65536]{2,1,0:T(2,128)(2,1)}), bf16[4,2,65536]{2,1,0:T(2,128)(2,1)S(1)}, u32[]{:S(2)}, u32[]{:S(2)}) async-start(bf16[4,2,65536]{2,1,0:T(2,128)(2,1)} %reshape.393), calls=%async_computation.2 | async-start | bytes 2097152 | tf_op jit(solution)/shard_map/all_to_all | solution.py:47
  153.3 232.5 %all-reduce.4.cloned.1.call-start = ((), (), s32[]{:S(2)}) async-start(), calls=%async_computation.7 | async-start | bytes 4194304 | tf_op jit(solution)/shard_map/psum | solution.py:73
  203.1 2.0 copy-start.4
  327.4 45.5 %all-to-all-start.3 = ((bf16[4,2,65536]{2,1,0:T(2,128)(2,1)}), bf16[4,2,65536]{2,1,0:T(2,128)(2,1)S(1)}, u32[]{:S(2)}, u32[]{:S(2)}) async-start(bf16[4,2,65536]{2,1,0:T(2,128)(2,1)} %reshape.395), calls=%async_computation.3 | async-start | bytes 2097152 | tf_op jit(solution)/shard_map/all_to_all | solution.py:58
  375.7 3.0 copy-start.7
  375.7 3.0 copy-start.9
  384.4 4.3 %copy-start.1 = (bf16[1,256,2048]{2,1,0:T(8,128)(2,1)S(1)}, bf16[1,256,2048]{2,1,0:T(8,128)(2,1)}, u32[]{:S(2)}) copy-start(bf16[1,256,2048]{2,1,0:T(8,128)(2,1)} %param.8) | copy-start | bytes 3145732
Sparse Core Ops, SparseCore 0:
  9.6 84.7 all-gather.1
  127.1 169.3 reduce-scatter.1
  299.6 69.1 all-reduce.3
where the time goes:
time: 402 us; the launch traced here: 395 us
  waiting for transfers between devices  110 us (27%)
  other arithmetic  102 us (25%)
  blocking collectives  75.9 us (19%)
  local copies, waits for them, and re-layouts  61.5 us (15%)
  starting transfers between devices  16.9 us (4%)
  matrix products  15 us (4%)
  between operations  14.3 us (4%)
    reduce_scatter x1, waiting for transfers between devices, body(): lax.psum_scatter(lax.dot_general(columns, activated, (((0,), (0,)), ((),...  81.4 us
    psum x1, blocking collectives, body(): grad_gain = lax.psum(gain_part, ('sp', 'dp'))  48.8 us
    unnamed x4, other arithmetic  38.5 us
    reduce_sum x4, other arithmetic, body(): jnp.sum(grad_heads * padded[:, offset:offset + length], axis=(0, 1))  32.4 us
    unnamed x39, local copies, waits for them, and re-layouts  28.2 us
    psum x1, blocking collectives, body(): grad_taps = lax.psum(jnp.stack(tap_terms), 'dp')  27.2 us
    all_to_all x1, waiting for transfers between devices, body(): lax.all_to_all(glu, 'sp', split_axis=2, concat_axis=1, tiled=True)  14.2 us
    all_to_all x1, waiting for transfers between devices, body(): lax.all_to_all(conv_out.astype(jnp.bfloat16), 'sp', split_axis=1, concat_...  13.4 us
  transfers between devices with their start and end apart: 7, of which 3 were waited for; matrix products, arithmetic and copies ran while one was open for 44% of the time, Pallas kernels for 0%

commit v1 on v0

--- a/solution.py
+++ b/solution.py
@@ -60,7 +60,7 @@
     ).astype(jnp.float32)
     grad_value = (grad_tokens * sig_gate).astype(jnp.bfloat16)
     grad_gate = (grad_tokens * value_wide * sig_gate * (1.0 - sig_gate)).astype(jnp.bfloat16)
-    grad_gain = lax.psum(gain_part, ("sp", "dp"))
+    grad_gain = lax.psum(lax.psum(gain_part, "dp"), "sp")
     columns = upstream_rows
     owned = lax.psum_scatter(
         lax.dot_general(

time: 402 us -> 449 us (1.12)
  waiting for transfers between devices: 110 us -> 212 us
  blocking collectives: 75.9 us -> 27 us
  other arithmetic: 102 us -> 87.9 us
  starting transfers between devices: 16.9 us -> 24.8 us
    psum x2 -> x1, blocking collectives: 75.9 us -> 10.9 us  [body(): grad_gain = lax.psum(lax.psum(gain_part, 'dp'), 'sp')]
    psum x1, waiting for transfers between devices: 0.01 us -> 50.9 us  [body(): grad_weight = lax.psum(owned, 'sp')]
    psum x0 -> x1, waiting for transfers between devices: none -> 29.5 us  [body(): grad_taps = lax.psum(jnp.stack(tap_terms), 'dp')]
    reduce_scatter x1, waiting for transfers between devices: 81.4 us -> 103 us  [body(): lax.psum_scatter(lax.dot_general(columns, activated, (((0,), (0,)), ((),...]
    all_to_all x0 -> x1, blocking collectives: none -> 16.1 us  [body(): lax.all_to_all(grad_conv_out.astype(jnp.bfloat16), 'sp', split_axis=2, co...]
    reduce_sum x4, other arithmetic: 32.4 us -> 19.5 us  [body(): jnp.sum(grad_heads * padded[:, offset:offset + length], axis=(0, 1))]
    all_to_all x1, starting transfers between devices: 5.38 us -> 16.2 us  [body(): lax.all_to_all(glu, 'sp', split_axis=2, concat_axis=1, tiled=True)]
    unnamed x39 -> x44, local copies, waits for them, and re-layouts: 28.2 us -> 27.1 us
  transfers between devices with their start and end apart: 7 -> 7, of which waited for: 3 -> 5; matrix products, arithmetic and copies ran while one was open for 44% -> 36% of each run, Pallas kernels for 0% -> 0%
where the time goes in v1:
time: 449 us; the launch traced here: 443 us
  waiting for transfers between devices  212 us (47%)
  other arithmetic  87.9 us (20%)
  local copies, waits for them, and re-layouts  61.5 us (14%)
  blocking collectives  27 us (6%)
  starting transfers between devices  24.8 us (6%)
  matrix products  15.6 us (3%)
  between operations  14.3 us (3%)
    reduce_scatter x1, waiting for transfers between devices, body(): lax.psum_scatter(lax.dot_general(columns, activated, (((0,), (0,)), ((),...  103 us
    psum x1, waiting for transfers between devices, body(): grad_weight = lax.psum(owned, 'sp')  50.9 us
    unnamed x4, other arithmetic  37.3 us
    psum x1, waiting for transfers between devices, body(): grad_taps = lax.psum(jnp.stack(tap_terms), 'dp')  29.5 us
    unnamed x44, local copies, waits for them, and re-layouts  27.1 us
    reduce_sum x4, other arithmetic, body(): jnp.sum(grad_heads * padded[:, offset:offset + length], axis=(0, 1))  19.5 us
    all_to_all x1, starting transfers between devices, body(): lax.all_to_all(glu, 'sp', split_axis=2, concat_axis=1, tiled=True)  16.2 us
    all_to_all x1, blocking collectives, body(): lax.all_to_all(grad_conv_out.astype(jnp.bfloat16), 'sp', split_axis=2, co...  16.1 us
  transfers between devices with their start and end apart: 7, of which 5 were waited for; matrix products, arithmetic and copies ran while one was open for 36% of the time, Pallas kernels for 0%

profile of v1, /device:TPU:0, one launch (start us, length us, event | category | flops | bytes accessed | tf_op | source)
XLA Modules:
  0.0 443.0 jit_solution(5670113685934083878)
XLA Ops:
  11.9 12.9 %copy.90 = bf16[1,256,2048]{1,0,2:T(2,128)(2,1)} copy(bf16[1,256,2048]{1,2,0:T(8,128)(2,1)S(1)} %fusion.1) | data formatting | bytes 2097152 | tf_op jit(solution)/shard_map/convert_element_type | solution.py:13
  25.4 11.6 %reduce.17 = bf16[2048,256]{1,0:T(8,128)(2,1)S(1)} reduce(bf16[2048,1,256]{2,1,0:T(2,128)(2,1)} %bitcast.178, bf16[]{:T(256)} %broadcast.201), dimensions={1}, to_apply=%bitcast.161.reduce_sub_computation | reduce | bytes 2097154
  38.7 16.2 %all-to-all-start = ((bf16[4,2,65536]{2,1,0:T(2,128)(2,1)}), bf16[4,2,65536]{2,1,0:T(2,128)(2,1)}, u32[]{:S(2)}, u32[]{:S(2)}) async-start(bf16[4,2,65536]{2,1,0:T(2,128)(2,1)} %reshape.389), calls=%async_computation | async-start | bytes 2097152 | tf_op jit(solution)/shard_map/all_to_all | solution.py:14
  55.0 14.5 %all-to-all-done = bf16[4,2,65536]{2,1,0:T(2,128)(2,1)} async-done(((bf16[4,2,65536]{2,1,0:T(2,128)(2,1)}), bf16[4,2,65536]{2,1,0:T(2,128)(2,1)}, u32[]{:S(2)}, u32[]{:S(2)}) %all-to-all-start) | async-done | bytes 1048608 | tf_op jit(solution)/shard_map/all_to_all | solution.py:14
  69.5 2.6 reshape.390
  76.1 8.0 %add_convert_fusion.1 = bf16[1,1024,512]{2,1,0:T(8,128)(2,1)S(1)} fusion(f32[1,1024,512]{2,1,0:T(8,128)S(1)} %bitcast.163, f32[512]{0:T(512)S(1)} %bitcast.207, f32[512]{0:T(512)S(1)} %bitcast.209, f32[512]{0:T(512)S(1)} %bitcast.213, f32[512]{0:T(512)S(1)} %bitcast.215, f32[512]{0:T(512)S(1)} %bitcast.217, f32[512]{0:T(512)S(1)} %bitcast.219, ...), kind=kLoop, calls=%fused_computation.88 | loop fusion | flops 32505856 | bytes 3209216 | tf_op jit(solution)/shard_map/convert_element_type | solution.py:23
  84.1 2.9 copy.89
  87.0 8.1 %reduce.18 = bf16[1024,512]{1,0:T(8,128)(2,1)S(1)} reduce(bf16[1024,1,512]{2,1,0:T(2,128)(2,1)} %bitcast.180, bf16[]{:T(256)} %broadcast.201), dimensions={1}, to_apply=%bitcast.160.reduce_sub_computation | reduce | bytes 2097154
  95.1 2.0 reshape.391
  97.1 4.3 all-to-all-start.1
  101.4 13.4 %all-to-all-done.1 = bf16[4,2,65536]{2,1,0:T(2,128)(2,1)} async-done(((bf16[4,2,65536]{2,1,0:T(2,128)(2,1)}), bf16[4,2,65536]{2,1,0:T(2,128)(2,1)}, u32[]{:S(2)}, u32[]{:S(2)}) %all-to-all-start.1) | async-done | bytes 1048608 | tf_op jit(solution)/shard_map/all_to_all | solution.py:22
  114.8 2.6 reshape.392
  126.2 2.3 copy.71
  128.4 9.3 %convolution_bitcast_fusion = f32[2048,2048]{0,1:T(8,128)} fusion(bf16[256,2048]{0,1:T(8,128)(2,1)} %bitcast.186, bf16[1,256,2048]{2,1,0:T(8,128)(2,1)S(1)} %copy-done), kind=kOutput, calls=%fused_computation | convolution fusion | flops 2147483648 | bytes 18874368 | tf_op jit(solution)/shard_map/dot_general | solution.py:66
  140.4 6.4 %multiply_reduce_fusion = (f32[2048]{0:T(1024)}, f32[256]{0:T(256)S(1)}, f32[256]{0:T(256)S(1)}, f32[256,2048]{1,0:T(8,128)S(1)}) fusion(f32[256,2048]{1,0:T(8,128)S(1)} %bitcast.176, f32[256]{0:T(256)S(1)} %broadcast_multiply_fusion.2, f32[256]{0:T(256)S(1)} %add_rsqrt_fusion, f32[2048]{0:T(1024)S(1)} %copy-done.13, ...), kind=kOutput, calls=%fused_computation.20 | convolution fusion | flops 2156393984 | bytes 13651968 | tf_op jit(solution)/shard_map/dot_general | solution.py:34
  149.2 10.6 %reduce.19 = bf16[2048,256]{1,0:T(8,128)(2,1)S(1)} reduce(bf16[2048,1,256]{2,1,0:T(2,128)(2,1)S(1)} %bitcast.182, bf16[]{:T(256)} %broadcast.201), dimensions={1}, to_apply=%bitcast.148.reduce_sub_computation | reduce | bytes 2097154
  160.1 16.1 %all_to_all.16 = bf16[4,2,65536]{2,1,0:T(2,128)(2,1)S(1)} all-to-all(bf16[4,2,65536]{2,1,0:T(2,128)(2,1)S(1)} %reshape.393), channel_id=1, replica_groups=mesh['sp'=4,'dp'=8] {'sp'}, dimensions={0} | all-to-all | bytes 2097152 | tf_op jit(solution)/shard_map/all_to_all | solution.py:47
  181.1 2.6 multiply_reduce_fusion.1
  183.8 11.8 %multiply_reduce_fusion.3 = (f32[512]{0:T(512)S(1)}, f32[512]{0:T(512)S(1)}, f32[512]{0:T(512)S(1)}, f32[512]{0:T(512)S(1)}, f32[512]{0:T(512)S(1)}, /*index=5*/...) fusion(f32[1,1024,512]{2,1,0:T(8,128)} %bitcast.164, ...), kind=kLoop, calls=%fused_computation.23 | loop fusion | flops 12576768 | bytes 4218880 | tf_op jit(solution)/shard_map/reduce_sum | solution.py:56
  195.6 5.0 %multiply_reduce_fusion.2 = (f32[512]{0:T(512)S(1)}, f32[512]{0:T(512)S(1)}, f32[512]{0:T(512)S(1)}, f32[512]{0:T(512)S(1)}, f32[512]{0:T(512)S(1)}, /*index=5*/...) fusion(f32[1,1024,512]{2,1,0:T(8,128)S(1)} %bitcast.165, ...), kind=kLoop, calls=%fused_computation.22 | loop fusion | flops 18865152 | bytes 4231168 | tf_op jit(solution)/shard_map/reduce_sum | solution.py:56
  200.6 2.5 stack.127
  203.4 102.7 %reduce-scatter.2.cloned.1.call-done = f32[256,2048]{0,1:T(8,128)} async-done(((f32[2048,2048]{0,1:T(8,128)}), f32[256,2048]{0,1:T(8,128)}) %reduce-scatter.2.cloned.1.call-update) | async-done | bytes 2097168 | tf_op jit(solution)/shard_map/reduce_scatter | solution.py:65
  306.2 8.0 %add_convert_fusion = bf16[1,1024,512]{2,1,0:T(8,128)(2,1)S(1)} fusion(f32[1,1024,512]{2,1,0:T(8,128)S(1)} %bitcast.162, f32[512]{0:T(512)S(1)} %bitcast.208, f32[512]{0:T(512)S(1)} %bitcast.210, f32[512]{0:T(512)S(1)} %bitcast.214, f32[512]{0:T(512)S(1)} %bitcast.216, f32[512]{0:T(512)S(1)} %bitcast.218, f32[512]{0:T(512)S(1)} %bitcast.220, ...), kind=kLoop, calls=%fused_computation.52 | loop fusion | flops 32505856 | bytes 3209216 | tf_op jit(solution)/shard_map/convert_element_type | solution.py:59
  315.8 7.0 %reduce.20 = bf16[1024,512]{1,0:T(8,128)(2,1)S(1)} reduce(bf16[1024,1,512]{2,1,0:T(2,128)(2,1)S(1)} %bitcast.179, bf16[]{:T(256)} %broadcast.201), dimensions={1}, to_apply=%bitcast.159.reduce_sub_computation | reduce | bytes 2097154
  324.8 3.6 all-to-all-start.3
  328.4 29.5 %all-reduce.8.cloned.1.call-done = (f32[31,512]{1,0:T(8,128)}, f32[2048]{0:T(1024)}) async-done(((f32[31,512]{1,0:T(8,128)}, f32[2048]{0:T(1024)}), (f32[31,512]{1,0:T(8,128)}, f32[2048]{0:T(1024)})) %all-reduce.8.cloned.1.call-update) | async-done | bytes 71696 | tf_op jit(solution)/shard_map/psum | solution.py:57
  357.9 10.9 %psum.30 = f32[2048]{0:T(1024)} all-reduce(f32[2048]{0:T(1024)} %get-tuple-element.69), channel_id=1, replica_groups=mesh['sp'=4,'dp'=8] {'sp'}, use_global_device_ids=true, to_apply=%region_40.41 | all-reduce | flops 2048 | bytes 16384 | tf_op jit(solution)/shard_map/psum | solution.py:63
  371.7 3.0 copy.70
  374.7 3.4 fusion.4
  378.1 2.3 copy.72
  381.8 50.9 %all-reduce.6.cloned.1.call-done = f32[256,2048]{0,1:T(8,128)} async-done(((f32[256,2048]{0,1:T(8,128)}), f32[256,2048]{0,1:T(8,128)}) %all-reduce.6.cloned.1.call-update) | async-done | bytes 2097168 | tf_op jit(solution)/shard_map/psum | solution.py:73
  432.7 2.9 copy.74
  (75 shorter events, 38.7 us)
Async XLA Ops:
  7.2 121.2 %copy-start = (bf16[1,256,2048]{2,1,0:T(8,128)(2,1)S(1)}, bf16[1,256,2048]{2,1,0:T(8,128)(2,1)}, u32[]{:S(2)}) copy-start(bf16[1,256,2048]{2,1,0:T(8,128)(2,1)} %param.8) | copy-start | bytes 3145732
  7.2 133.3 %all-gather.2.cloned.1.call-start = ((), (), s32[]{:S(2)}) async-start(), calls=%async_computation.5 | async-start | bytes 9437184 | tf_op jit(solution)/shard_map/all_gather | solution.py:36
  9.4 2.5 copy-start.7
  11.3 13.5 %copy-start.9 = (bf16[1,256,2048]{1,2,0:T(8,128)(2,1)}, bf16[1,256,2048]{1,2,0:T(8,128)(2,1)S(1)}, u32[]{:S(2)}) copy-start(bf16[1,256,2048]{1,2,0:T(8,128)(2,1)S(1)} %copy.57) | copy-start | bytes 3145732
  37.0 17.9 %copy-start.12 = (f32[31,512]{1,0:T(8,128)S(1)}, f32[31,512]{1,0:T(8,128)}, u32[]{:S(2)}) copy-start(f32[31,512]{1,0:T(8,128)} %param.9) | copy-start | bytes 190468
  38.7 30.8 %all-to-all-start = ((bf16[4,2,65536]{2,1,0:T(2,128)(2,1)}), bf16[4,2,65536]{2,1,0:T(2,128)(2,1)}, u32[]{:S(2)}, u32[]{:S(2)}) async-start(bf16[4,2,65536]{2,1,0:T(2,128)(2,1)} %reshape.389), calls=%async_computation | async-start | bytes 2097152 | tf_op jit(solution)/shard_map/all_to_all | solution.py:14
  72.1 2.0 copy-start.4
  76.1 10.9 %copy-start.2 = (f32[1,4,256,512]{3,2,1,0:T(8,128)}, f32[1,4,256,512]{3,2,1,0:T(8,128)S(1)}, u32[]{:S(2)}) copy-start(f32[1,4,256,512]{3,2,1,0:T(8,128)S(1)} %copy.60) | copy-start | bytes 6291460
  95.1 6.3 %copy-start.13 = (f32[2048]{0:T(1024)S(1)}, f32[2048]{0:T(1024)}, u32[]{:S(2)}) copy-start(f32[2048]{0:T(1024)} %param.10) | copy-start | bytes 24580
  97.1 17.7 %all-to-all-start.1 = ((bf16[4,2,65536]{2,1,0:T(2,128)(2,1)}), bf16[4,2,65536]{2,1,0:T(2,128)(2,1)}, u32[]{:S(2)}, u32[]{:S(2)}) async-start(bf16[4,2,65536]{2,1,0:T(2,128)(2,1)} %reshape.391), calls=%async_computation.1 | async-start | bytes 2097152 | tf_op jit(solution)/shard_map/all_to_all | solution.py:22
  101.4 204.8 %reduce-scatter.2.cloned.1.call-start = ((), (), s32[]{:S(2)}) async-start(), calls=%async_computation.6 | async-start | bytes 18874368 | tf_op jit(solution)/shard_map/reduce_scatter | solution.py:65
  117.4 1.3 copy-start.6
  137.7 220.2 %all-reduce.8.cloned.1.call-start = ((), (), s32[]{:S(2)}) async-start(), calls=%async_computation.8 | async-start | bytes 147456 | tf_op jit(solution)/shard_map/psum | solution.py:57
  177.2 2.0 copy-start.5
  183.8 11.8 %copy-start.3 = (f32[1,4,256,512]{3,2,1,0:T(8,128)S(1)}, f32[1,4,256,512]{3,2,1,0:T(8,128)}, u32[]{:S(2)}) copy-start(f32[1,4,256,512]{3,2,1,0:T(8,128)} %copy-done.2) | copy-start | bytes 6291460
  203.2 229.6 %all-reduce.6.cloned.1.call-start = ((), (), s32[]{:S(2)}) async-start(), calls=%async_computation.7 | async-start | bytes 4194304 | tf_op jit(solution)/shard_map/psum | solution.py:73
  324.8 44.0 %all-to-all-start.3 = ((bf16[4,2,65536]{2,1,0:T(2,128)(2,1)}), bf16[4,2,65536]{2,1,0:T(2,128)(2,1)S(1)}, u32[]{:S(2)}, u32[]{:S(2)}) async-start(bf16[4,2,65536]{2,1,0:T(2,128)(2,1)} %reshape.395), calls=%async_computation.3 | async-start | bytes 2097152 | tf_op jit(solution)/shard_map/all_to_all | solution.py:58
  371.7 3.0 copy-start.8
  371.7 3.0 copy-start.10
  380.4 55.9 %copy-start.1 = (bf16[1,256,2048]{2,1,0:T(8,128)(2,1)S(1)}, bf16[1,256,2048]{2,1,0:T(8,128)(2,1)}, u32[]{:S(2)}) copy-start(bf16[1,256,2048]{2,1,0:T(8,128)(2,1)} %param.8) | copy-start | bytes 3145732
  381.8 53.8 %copy-start.11 = (f32[31,512]{1,0:T(8,128)S(1)}, f32[31,512]{1,0:T(8,128)}, u32[]{:S(2)}) copy-start(f32[31,512]{1,0:T(8,128)} %get-tuple-element.108) | copy-start | bytes 190468
Sparse Core Ops, SparseCore 0:
  9.6 84.7 all-gather.1
  137.8 168.2 reduce-scatter.1
  309.1 48.7 all-reduce.7
  360.9 71.8 all-reduce.5
